TPU v7x, 32 devices: a whole 2x2x4 slice. The times are simulated.
32 devices in a mesh: fs: 8 (over z, core), tp: 4 (over y, x).
Axes of the slice: x: 2, y: 2, z: 4, core: 2. Of those that a mesh axis runs over, the one named last changes fastest.
Arguments:
- tokens: bfloat16 [1024, 2048], P('fs'), may hold values from -6 to 6
- experts: int32 [1024, 4], P('fs'), may hold values from 0 to 7, all different within a row; in each aligned block of 128 rows (0 to 127, 128 to 255, ...) at most 96 rows name the same one
- routing: float32 [1024, 4], P('fs'), may hold values from 0.05 to 0.6
- norm_gain: float32 [2048], replicated, may hold values from 0.1 to 1.9
- gate_master: float32 [8, 2048, 2048], P(None, 'fs', 'tp'), may hold values from -0.625 to 0.625
- linear_master: float32 [8, 2048, 2048], P(None, 'fs', 'tp'), may hold values from -0.625 to 0.625
- down_weight: bfloat16 [8, 2048, 2048], P('fs', None, 'tp'), may hold values from -0.013671875 to 0.013671875
Outputs:
- gate_out: bfloat16 [8, 2048, 2048], P('fs', None, 'tp')
- linear_out: bfloat16 [8, 2048, 2048], P('fs', None, 'tp')
- expert_mix: bfloat16 [1024, 2048], P('fs', 'tp')
Inputs may be any that keep to these rules, and one draw needn't show every extreme that they name: Each row names 4 different experts; within the rows of one index of fs (aligned blocks of 128 rows) no expert is named by more than 96 rows, and in some blocks some expert is named by exactly 96; every expert is named somewhere.
All inputs are finite; a program needn't handle non-finite values.
Results may differ from a plain program's by a relative error of at most 0.023.
Values may be sent and summed in bfloat16 or wider, within the bound.
A program may use at most 64 MiB of HBM per device.

v0:
```python
import jax
import jax.numpy as jnp
from jax import lax
from jax.sharding import PartitionSpec as P

clamp_limit = 7.0
gate_slope = 1.702


def on_device(tokens, experts, routing, norm_gain, gate_master, linear_master, down_weight):
    tok_count, top_count = experts.shape
    expert_count = gate_master.shape[0]
    width = tokens.shape[1]
    capacity = 3 * tok_count * top_count // (2 * expert_count)
    moved_gate, moved_linear = (
        lax.all_to_all(
            gate_master.astype(jnp.bfloat16), "fs", split_axis=0, concat_axis=1, tiled=True
        ).astype(gate_master.dtype),
        lax.all_to_all(
            linear_master.astype(jnp.bfloat16), "fs", split_axis=0, concat_axis=1, tiled=True
        ).astype(linear_master.dtype),
    )
    gate_out = (moved_gate * norm_gain[None, :, None]).astype(jnp.bfloat16)
    linear_out = (moved_linear * norm_gain[None, :, None]).astype(jnp.bfloat16)
    flat_ids = experts.reshape(-1)
    one_hot = (flat_ids[:, None] == jnp.arange(expert_count, dtype=jnp.int32)[None, :]).astype(
        jnp.int32
    )
    slot_rank = jnp.sum((jnp.cumsum(one_hot, axis=0) - one_hot) * one_hot, axis=1)
    slot_index = flat_ids * capacity + slot_rank
    owner = jnp.arange(tok_count * top_count, dtype=jnp.int32) // top_count
    slot_token = (
        jnp.full((expert_count * capacity,), tok_count, jnp.int32).at[slot_index].set(owner)
    )
    padded = jnp.concatenate([tokens, jnp.zeros((1, width), tokens.dtype)], axis=0)
    sender = padded[slot_token].reshape(expert_count, capacity, width)
    gate_local = gate_out[0]
    linear_local = linear_out[0]
    down_local = down_weight[0]
    item_rows = lax.all_to_all(sender, "fs", split_axis=0, concat_axis=0, tiled=True)
    flat_rows = item_rows.reshape(-1, width)
    pre_gate = jnp.dot(flat_rows, gate_local, preferred_element_type=jnp.float32)
    pre_linear = jnp.dot(flat_rows, linear_local, preferred_element_type=jnp.float32)
    clamped = jnp.minimum(pre_gate, clamp_limit)
    active = (
        clamped
        * jax.nn.sigmoid(gate_slope * clamped)
        * (jnp.clip(pre_linear, -clamp_limit, clamp_limit) + 1.0)
    ).astype(jnp.bfloat16)
    partial_value = lax.dot_general(
        active, down_local, (((1,), (1,)), ((), ())), preferred_element_type=jnp.float32
    ).reshape(item_rows.shape)
    results = partial_value.astype(jnp.bfloat16)
    summed = lax.psum_scatter(results, "tp", scatter_dimension=2, tiled=True).astype(jnp.float32)
    returned = lax.all_to_all(
        summed.astype(jnp.bfloat16), "fs", split_axis=0, concat_axis=0, tiled=True
    ).astype(summed.dtype)
    picked = returned.reshape(expert_count * capacity, -1)[slot_index].reshape(
        tok_count, top_count, -1
    )
    expert_mix = jnp.sum(routing[:, :, None] * picked, axis=1).astype(jnp.bfloat16)
    return (gate_out, linear_out, expert_mix)


def solution(mesh):
    placed = (
        P("fs", None),
        P("fs", None),
        P("fs", None),
        P(),
        P(None, "fs", "tp"),
        P(None, "fs", "tp"),
        P("fs", None, "tp"),
    )
    return jax.shard_map(
        on_device,
        mesh=mesh,
        in_specs=placed,
        out_specs=(P("fs", None, "tp"), P("fs", None, "tp"), P("fs", "tp")),
        check_vma=False,
    )
```

profile of v0, /device:TPU:0, one launch (start us, length us, event | category | flops | bytes accessed | tf_op | source)
XLA Modules:
  0.0 293.1 jit_solution(636927419273226423)
XLA Ops:
  7.2 3.9 %convert_element_type.149 = bf16[8,256,512]{2,1,0:T(8,128)(2,1)} convert(f32[8,256,512]{2,1,0:T(8,128)} %param.11) | non-fusion elementwise | flops 1048576 | bytes 6291456 | tf_op jit(solution)/shard_map/convert_element_type | solution.py:17
  11.1 6.4 %all-to-all-start = ((bf16[8,256,512]{2,1,0:T(8,128)(2,1)}), bf16[8,256,512]{2,1,0:T(8,128)(2,1)}, u32[]{:S(2)}, u32[]{:S(2)}) async-start(bf16[8,256,512]{2,1,0:T(8,128)(2,1)} %convert_element_type.149), calls=%async_computation | async-start | bytes 4194304 | tf_op jit(solution)/shard_map/all_to_all | solution.py:16
  17.5 3.8 %convert_element_type.153 = bf16[8,256,512]{2,1,0:T(8,128)(2,1)} convert(f32[8,256,512]{2,1,0:T(8,128)} %param.12) | non-fusion elementwise | flops 1048576 | bytes 6291456 | tf_op jit(solution)/shard_map/convert_element_type | solution.py:20
  21.2 45.4 %all-to-all-done = bf16[8,256,512]{2,1,0:T(8,128)(2,1)} async-done(((bf16[8,256,512]{2,1,0:T(8,128)(2,1)}), bf16[8,256,512]{2,1,0:T(8,128)(2,1)}, u32[]{:S(2)}, u32[]{:S(2)}) %all-to-all-start) | async-done | bytes 2097184 | tf_op jit(solution)/shard_map/all_to_all | solution.py:16
  66.6 4.4 %all-to-all-start.1 = ((bf16[8,256,512]{2,1,0:T(8,128)(2,1)}), bf16[8,256,512]{2,1,0:T(8,128)(2,1)}, u32[]{:S(2)}, u32[]{:S(2)}) async-start(bf16[8,256,512]{2,1,0:T(8,128)(2,1)} %convert_element_type.153), calls=%async_computation.1 | async-start | bytes 4194304 | tf_op jit(solution)/shard_map/all_to_all | solution.py:19
  71.0 0.1 copy.13
  71.1 0.1 eq.29
  71.2 0.1 eq.25
  71.3 0.1 copy.12
  71.4 0.1 mul.109
  71.5 1.1 reduce-window.6
  72.7 0.2 slice_reduce_fusion
  73.0 0.1 fusion.14
  73.1 2.4 scatter_custom_fusion
  75.6 4.2 %gather_fusion = bf16[768,2048]{1,0:T(8,128)(2,1)} fusion(bf16[129,2048]{1,0:T(8,128)(2,1)S(1)} %concatenate.3, s32[1024]{0:T(1024)S(1)} %pad_clamp_fusion.1), kind=kCustom, calls=%fused_computation | custom fusion | bytes 6294528 | tf_op jit(solution)/shard_map/gather | solution.py:36
  79.8 40.2 %all-to-all-done.1 = bf16[8,256,512]{2,1,0:T(8,128)(2,1)} async-done(((bf16[8,256,512]{2,1,0:T(8,128)(2,1)}), bf16[8,256,512]{2,1,0:T(8,128)(2,1)}, u32[]{:S(2)}, u32[]{:S(2)}) %all-to-all-start.1) | async-done | bytes 2097184 | tf_op jit(solution)/shard_map/all_to_all | solution.py:19
  120.0 4.5 %all-to-all-start.2 = ((bf16[8,96,2048]{2,1,0:T(8,128)(2,1)}), bf16[8,96,2048]{2,1,0:T(8,128)(2,1)}, u32[]{:S(2)}, u32[]{:S(2)}) async-start(bf16[8,96,2048]{2,1,0:T(8,128)(2,1)} %bitcast.47), calls=%async_computation.2 | async-start | bytes 6291456 | tf_op jit(solution)/shard_map/all_to_all | solution.py:40
  124.5 4.1 %convert_element_type.170 = f32[8,256,512]{2,1,0:T(8,128)} convert(bf16[8,256,512]{2,1,0:T(8,128)(2,1)} %all-to-all-done) | non-fusion elementwise | flops 1048576 | bytes 6291456 | tf_op jit(solution)/shard_map/convert_element_type | solution.py:18
  128.6 4.2 %convert_element_type.171 = f32[8,256,512]{2,1,0:T(8,128)} convert(bf16[8,256,512]{2,1,0:T(8,128)(2,1)} %all-to-all-done.1) | non-fusion elementwise | flops 1048576 | bytes 6291456 | tf_op jit(solution)/shard_map/convert_element_type | solution.py:21
  132.8 63.2 %all-to-all-done.2 = bf16[8,96,2048]{2,1,0:T(8,128)(2,1)} async-done(((bf16[8,96,2048]{2,1,0:T(8,128)(2,1)}), bf16[8,96,2048]{2,1,0:T(8,128)(2,1)}, u32[]{:S(2)}, u32[]{:S(2)}) %all-to-all-start.2) | async-done | bytes 3145760 | tf_op jit(solution)/shard_map/all_to_all | solution.py:40
  196.0 5.1 %fusion.3 = f32[768,512]{1,0:T(8,128)S(1)} fusion(bf16[768,2048]{1,0:T(8,128)(2,1)} %bitcast.7, f32[1,2048,1,1,1,1,512]{6,1,5,4,3,2,0:T(8,128)} %bitcast.43, f32[2048]{0:T(1024)S(1)} %copy-done.4), kind=kOutput, calls=%fused_computation.11 | convolution fusion | flops 1612709888 | bytes 8921088 | tf_op jit(solution)/shard_map/dot_general | solution.py:42
  201.2 4.1 %multiply_convert_fusion.2 = bf16[768,512]{1,0:T(8,128)(2,1)S(1)} fusion(f32[768,512]{1,0:T(8,128)S(1)} %fusion.3, bf16[768,2048]{1,0:T(8,128)(2,1)} %bitcast.7, f32[1,2048,1,1,1,1,512]{6,1,5,4,3,2,0:T(8,128)S(1)} %bitcast.46, f32[2048]{0:T(1024)S(1)} %copy-done.4), kind=kOutput, calls=%fused_computation.17 | convolution fusion | flops 1616642048 | bytes 9707520 | tf_op jit(solution)/shard_map/dot_general | solution.py:43
  205.3 3.6 %convolution_convert_fusion = bf16[8,96,2048]{2,1,0:T(8,128)(2,1)} fusion(bf16[8,96,512]{2,1,0:T(8,128)(2,1)S(1)} %bitcast.51, bf16[1,2048,512]{2,1,0:T(8,128)(2,1)S(1)} %copy-done), kind=kOutput, calls=%fused_computation.9 | convolution fusion | flops 1612185600 | bytes 6029312 | tf_op jit(solution)/shard_map/dot_general | solution.py:50
  209.0 43.0 %reduce-scatter.2.cloned.1.call-done = bf16[8,96,512]{2,1,0:T(8,128)(2,1)} async-done(((bf16[8,96,2048]{2,1,0:T(8,128)(2,1)}), bf16[8,96,512]{2,1,0:T(8,128)(2,1)}) %reduce-scatter.2.cloned.1.call-update) | async-done | bytes 786448 | tf_op jit(solution)/shard_map/reduce_scatter | solution.py:54
  251.9 4.6 %all-to-all-start.3 = ((bf16[8,96,512]{2,1,0:T(8,128)(2,1)}), bf16[8,96,512]{2,1,0:T(8,128)(2,1)S(1)}, u32[]{:S(2)}, u32[]{:S(2)}) async-start(bf16[8,96,512]{2,1,0:T(8,128)(2,1)} %reduce-scatter.2.cloned.1.call-done), calls=%async_computation.4 | async-start | bytes 1572864 | tf_op jit(solution)/shard_map/all_to_all | solution.py:55
  256.5 0.1 copy.11
  256.7 6.0 %fusion = (bf16[1,2048,512]{2,1,0:T(8,128)(2,1)}, bf16[1,2048,512]{2,1,0:T(8,128)(2,1)}) fusion(f32[2048]{0:T(1024)S(1)} %copy-done.4, f32[1,2048,512]{2,1,0:T(8,128)} %bitcast.45, f32[1,2048,512]{2,1,0:T(8,128)} %bitcast.44), kind=kLoop, calls=%fused_computation.4 | loop fusion | flops 4194304 | bytes 12591104 | tf_op jit(solution)/shard_map/convert_element_type | solution.py:24
  262.7 14.8 %all-to-all-done.3 = bf16[8,96,512]{2,1,0:T(8,128)(2,1)S(1)} async-done(((bf16[8,96,512]{2,1,0:T(8,128)(2,1)}), bf16[8,96,512]{2,1,0:T(8,128)(2,1)S(1)}, u32[]{:S(2)}, u32[]{:S(2)}) %all-to-all-start.3) | async-done | bytes 786464 | tf_op jit(solution)/shard_map/all_to_all | solution.py:55
  277.5 1.4 bitcast_convert_fusion
  278.9 3.4 %gather_fusion.1 = f32[512,512]{1,0:T(8,128)S(1)} fusion(f32[768,512]{1,0:T(8,128)} %bitcast_convert_fusion, s32[1024]{0:T(1024)S(1)} %pad_clamp_fusion), kind=kCustom, calls=%fused_computation.1 | custom fusion | bytes 2099200 | tf_op jit(solution)/shard_map/gather | solution.py:58
  282.3 1.3 reshape.249
  283.6 2.6 multiply_reduce_fusion
  (24 shorter events, 0.2 us)
Async XLA Ops:
  7.2 198.1 %copy-start = (bf16[1,2048,512]{2,1,0:T(8,128)(2,1)S(1)}, bf16[1,2048,512]{2,1,0:T(8,128)(2,1)}, u32[]{:S(2)}) copy-start(bf16[1,2048,512]{2,1,0:T(8,128)(2,1)} %param.13) | copy-start | bytes 6291460
  11.1 55.5 %all-to-all-start = ((bf16[8,256,512]{2,1,0:T(8,128)(2,1)}), bf16[8,256,512]{2,1,0:T(8,128)(2,1)}, u32[]{:S(2)}, u32[]{:S(2)}) async-start(bf16[8,256,512]{2,1,0:T(8,128)(2,1)} %convert_element_type.149), calls=%async_computation | async-start | bytes 4194304 | tf_op jit(solution)/shard_map/all_to_all | solution.py:16
  21.2 49.7 %copy-start.3 = (s32[128,4]{0,1:T(4,128)S(1)}, s32[128,4]{0,1:T(4,128)}, u32[]{:S(2)}) copy-start(s32[128,4]{0,1:T(4,128)} %param.8) | copy-start | bytes 6148
  21.2 51.7 %copy-start.2 = (bf16[128,2048]{1,0:T(8,128)(2,1)S(1)}, bf16[128,2048]{1,0:T(8,128)(2,1)}, u32[]{:S(2)}) copy-start(bf16[128,2048]{1,0:T(8,128)(2,1)} %param.7) | copy-start | bytes 1572868
  66.6 53.4 %all-to-all-start.1 = ((bf16[8,256,512]{2,1,0:T(8,128)(2,1)}), bf16[8,256,512]{2,1,0:T(8,128)(2,1)}, u32[]{:S(2)}, u32[]{:S(2)}) async-start(bf16[8,256,512]{2,1,0:T(8,128)(2,1)} %convert_element_type.153), calls=%async_computation.1 | async-start | bytes 4194304 | tf_op jit(solution)/shard_map/all_to_all | solution.py:19
  120.0 76.0 %all-to-all-start.2 = ((bf16[8,96,2048]{2,1,0:T(8,128)(2,1)}), bf16[8,96,2048]{2,1,0:T(8,128)(2,1)}, u32[]{:S(2)}, u32[]{:S(2)}) async-start(bf16[8,96,2048]{2,1,0:T(8,128)(2,1)} %bitcast.47), calls=%async_computation.2 | async-start | bytes 6291456 | tf_op jit(solution)/shard_map/all_to_all | solution.py:40
  124.5 127.4 %reduce-scatter.2.cloned.1.call-start = ((), (), s32[]{:S(2)}) async-start(), calls=%async_computation.5 | async-start | bytes 3932160 | tf_op jit(solution)/shard_map/reduce_scatter | solution.py:54
  128.6 67.4 %copy-start.4 = (f32[2048]{0:T(1024)S(1)}, f32[2048]{0:T(1024)}, u32[]{:S(2)}) copy-start(f32[2048]{0:T(1024)} %param.10) | copy-start | bytes 24580
  196.0 5.2 %copy-start.1 = (f32[8,256,512]{2,1,0:T(8,128)S(1)}, f32[8,256,512]{2,1,0:T(8,128)}, u32[]{:S(2)}) copy-start(f32[8,256,512]{2,1,0:T(8,128)} %convert_element_type.171) | copy-start | bytes 12582916
  208.9 47.6 %copy-start.5 = (f32[128,4]{0,1:T(4,128)S(1)}, f32[128,4]{0,1:T(4,128)}, u32[]{:S(2)}) copy-start(f32[128,4]{0,1:T(4,128)} %param.9) | copy-start | bytes 6148
  251.9 25.6 %all-to-all-start.3 = ((bf16[8,96,512]{2,1,0:T(8,128)(2,1)}), bf16[8,96,512]{2,1,0:T(8,128)(2,1)S(1)}, u32[]{:S(2)}, u32[]{:S(2)}) async-start(bf16[8,96,512]{2,1,0:T(8,128)(2,1)} %reduce-scatter.2.cloned.1.call-done), calls=%async_computation.4 | async-start | bytes 1572864 | tf_op jit(solution)/shard_map/all_to_all | solution.py:55
Sparse Core Ops, SparseCore 0:
  209.1 42.8 reduce-scatter.1
where the time goes:
time: 294 us; the launch traced here: 293 us
  waiting for transfers between devices  207 us (70%)
  other arithmetic  27.3 us (9%)
  starting transfers between devices  19.9 us (7%)
  between operations  14.2 us (5%)
  matrix products  12.9 us (4%)
  local copies, waits for them, and re-layouts  12.4 us (4%)
    all_to_all x1, waiting for transfers between devices, on_device(): lax.all_to_all(sender, 'fs', split_axis=0, concat_axis=0, tiled=True)  63.2 us
    all_to_all x1, waiting for transfers between devices, on_device(): lax.all_to_all(gate_master.astype(jnp.bfloat16), 'fs', split_axis=0, conc...  45.4 us
    reduce_scatter x1, waiting for transfers between devices, on_device(): lax.psum_scatter(results, 'tp', scatter_dimension=2, tiled=True)  43 us
    all_to_all x1, waiting for transfers between devices, on_device(): lax.all_to_all(linear_master.astype(jnp.bfloat16), 'fs', split_axis=0, co...  40.2 us
    all_to_all x1, waiting for transfers between devices, on_device(): lax.all_to_all(summed.astype(jnp.bfloat16), 'fs', split_axis=0, concat_ax...  14.8 us
    convert_element_type x2, other arithmetic, on_device(): moved_gate, moved_linear = (lax.all_to_all(gate_master.astype(jnp.bfloat1...  8.24 us
    all_to_all x1, starting transfers between devices, on_device(): lax.all_to_all(gate_master.astype(jnp.bfloat16), 'fs', split_axis=0, conc...  6.35 us
    convert_element_type x1, other arithmetic, on_device(): linear_out = (moved_linear * norm_gain[None, :, None]).astype(jnp.bfloat16)  6 us
  transfers between devices with their start and end apart: 5, of which 5 were waited for; matrix products, arithmetic and copies ran while one was open for 9% of the time, Pallas kernels for 0%

commit v1 on v0

v1 whole, which is shorter than its diff:
```python
import jax
import jax.numpy as jnp
from jax import lax
from jax.sharding import PartitionSpec as P

clamp_limit = 7.0
gate_slope = 1.702


def solution(mesh):
    n_fs, n_tp = mesh.shape["fs"], mesh.shape["tp"]

    def on_device(tokens, experts, routing, norm_gain, gate_master, linear_master, down_weight):
        expert_count, depth, _ = gate_master.shape
        width = tokens.shape[1]
        fs, tp = lax.axis_index("fs"), lax.axis_index("tp")
        cols = width // n_tp
        mine = lax.dynamic_slice_in_dim(tokens, tp * cols, cols, axis=1)
        quarter = lax.all_gather(mine, "fs", axis=0, tiled=True)
        everyone = lax.all_gather(quarter, "tp", axis=1, tiled=True)
        choice = experts[:, :, None] == jnp.arange(expert_count, dtype=jnp.int32)[None, None, :]
        share = jnp.sum(jnp.where(choice, routing[:, :, None], 0.0), axis=1)
        shares = lax.all_gather(share, "fs", axis=0, tiled=True)
        share_mine = lax.dynamic_slice_in_dim(shares, fs, 1, axis=1)
        gain = lax.dynamic_slice_in_dim(norm_gain, fs * depth, depth, axis=0)[None, :, None]
        gate_out, linear_out = (
            lax.all_to_all(
                (master * gain).astype(jnp.bfloat16), "fs", split_axis=0, concat_axis=1, tiled=True
            )
            for master in (gate_master, linear_master)
        )
        pre_gate = jnp.dot(everyone, gate_out[0], preferred_element_type=jnp.float32)
        pre_linear = jnp.dot(everyone, linear_out[0], preferred_element_type=jnp.float32)
        clamped = jnp.minimum(pre_gate, clamp_limit)
        active = (
            clamped
            * jax.nn.sigmoid(gate_slope * clamped)
            * (jnp.clip(pre_linear, -clamp_limit, clamp_limit) + 1.0)
        ).astype(jnp.bfloat16)
        part = lax.dot_general(
            active, down_weight[0], (((1,), (1,)), ((), ())), preferred_element_type=jnp.float32
        )
        part = (part * share_mine).astype(jnp.bfloat16)
        summed = lax.psum_scatter(part, "tp", scatter_dimension=1, tiled=True)
        mixed = lax.psum_scatter(summed, "fs", scatter_dimension=0, tiled=True)
        return (gate_out, linear_out, mixed)

    placed = (
        P("fs", None),
        P("fs", None),
        P("fs", None),
        P(),
        P(None, "fs", "tp"),
        P(None, "fs", "tp"),
        P("fs", None, "tp"),
    )
    return jax.shard_map(
        on_device,
        mesh=mesh,
        in_specs=placed,
        out_specs=(P("fs", None, "tp"), P("fs", None, "tp"), P("fs", "tp")),
        check_vma=False,
    )
```

time: 294 us -> 256 us (0.87)
  waiting for transfers between devices: 207 us -> 143 us
  blocking collectives: 0 us -> 55 us
  other arithmetic: 27.3 us -> 6.81 us
  starting transfers between devices: 19.9 us -> 11 us
  matrix products: 12.9 us -> 16.8 us
  local copies, waits for them, and re-layouts: 12.4 us -> 8.59 us
    all_to_all x4 -> x2, waiting for transfers between devices: 164 us -> 37.4 us  [on_device(): lax.all_to_all((master * gain).astype(jnp.bfloat16), 'fs', split_axis=0,...]
    all_gather x0 -> x1, blocking collectives: none -> 55 us  [on_device(): shares = lax.all_gather(share, 'fs', axis=0, tiled=True)]
    reduce_scatter x1 -> x2, waiting for transfers between devices: 43 us -> 88.2 us  [the longest x1 52.8 us: on_device(): summed = lax.psum_scatter(part, 'tp', scatter_dimension=1, tiled=True)]
    all_gather x0 -> x2, waiting for transfers between devices: none -> 17.5 us  [the longest x1 17.5 us: on_device(): quarter = lax.all_gather(mine, 'fs', axis=0, tiled=True)]
    convert_element_type x6 -> x1, other arithmetic: 21.9 us -> 6.8 us  [on_device(): (master * gain).astype(jnp.bfloat16)]
    all_to_all x4 -> x2, starting transfers between devices: 19.8 us -> 10.8 us  [on_device(): lax.all_to_all((master * gain).astype(jnp.bfloat16), 'fs', split_axis=0,...]
    gather x2 -> x0, local copies, waits for them, and re-layouts: 7.67 us -> none  [the longest x1 4.24 us: on_device(): sender = padded[slot_token].reshape(expert_count, capacity, width)]
    unnamed x14 -> x8, local copies, waits for them, and re-layouts: 0.25 us -> 6.1 us
  transfers between devices with their start and end apart: 5 -> 6, of which waited for: 5 -> 4; matrix products, arithmetic and copies ran while one was open for 9% -> 6% of each run, Pallas kernels for 0% -> 0%
where the time goes in v1:
time: 256 us; the launch traced here: 255 us
  waiting for transfers between devices  143 us (56%)
  blocking collectives  55 us (21%)
  matrix products  16.8 us (7%)
  between operations  13.8 us (5%)
  starting transfers between devices  11 us (4%)
  local copies, waits for them, and re-layouts  8.59 us (3%)
  other arithmetic  6.81 us (3%)
    all_gather x1, blocking collectives, on_device(): shares = lax.all_gather(share, 'fs', axis=0, tiled=True)  55 us
    reduce_scatter x1, waiting for transfers between devices, on_device(): summed = lax.psum_scatter(part, 'tp', scatter_dimension=1, tiled=True)  52.8 us
    all_to_all x2, waiting for transfers between devices, on_device(): lax.all_to_all((master * gain).astype(jnp.bfloat16), 'fs', split_axis=0,...  37.4 us
    reduce_scatter x1, waiting for transfers between devices, on_device(): mixed = lax.psum_scatter(summed, 'fs', scatter_dimension=0, tiled=True)  35.4 us
    all_gather x1, waiting for transfers between devices, on_device(): quarter = lax.all_gather(mine, 'fs', axis=0, tiled=True)  17.5 us
    all_to_all x2, starting transfers between devices, on_device(): lax.all_to_all((master * gain).astype(jnp.bfloat16), 'fs', split_axis=0,...  10.8 us
    dot_general x1, matrix products, on_device(): lax.dot_general(active, down_weight[0], (((1,), (1,)), ((), ())), preferr...  10.3 us
    convert_element_type x1, other arithmetic, on_device(): (master * gain).astype(jnp.bfloat16)  6.8 us
  transfers between devices with their start and end apart: 6, of which 4 were waited for; matrix products, arithmetic and copies ran while one was open for 6% of the time, Pallas kernels for 0%

profile of v1, /device:TPU:0, one launch (start us, length us, event | category | flops | bytes accessed | tf_op | source)
XLA Modules:
  0.0 255.2 jit_solution(7410514343636466735)
XLA Ops:
  7.2 0.0 copy-start
  7.2 0.0 all-gather.3.cloned.1.call-start
  7.2 1.7 constant_dynamic-slice_fusion.1
  8.9 0.0 all-gather.3.cloned.1.call-update
  9.0 0.8 dynamic_slice.9
  9.7 6.8 %multiply_convert_fusion.1 = (bf16[8,256,512]{2,1,0:T(8,128)(2,1)}, bf16[8,256,512]{2,1,0:T(8,128)(2,1)}) fusion(f32[8,256,512]{2,1,0:T(8,128)} %param.12, f32[256]{0:T(256)S(1)} %dynamic_slice.9, f32[8,256,512]{2,1,0:T(8,128)} %param.11), kind=kLoop, calls=%fused_computation.1 | loop fusion | flops 4194304 | bytes 12583936 | tf_op jit(solution)/shard_map/convert_element_type | solution.py:28
  16.5 6.4 %all-to-all-start.1 = ((bf16[8,256,512]{2,1,0:T(8,128)(2,1)}), bf16[8,256,512]{2,1,0:T(8,128)(2,1)}, u32[]{:S(2)}, u32[]{:S(2)}) async-start(bf16[8,256,512]{2,1,0:T(8,128)(2,1)} %get-tuple-element.3), calls=%async_computation.1 | async-start | bytes 4194304 | tf_op jit(solution)/shard_map/all_to_all | solution.py:27
  22.9 0.0 all-gather.5.cloned.1.call-start
  22.9 17.5 %all-gather.3.cloned.1.call-done = bf16[1024,512]{1,0:T(8,128)(2,1)} async-done(((bf16[128,512]{1,0:T(8,128)(2,1)}), bf16[1024,512]{1,0:T(8,128)(2,1)}) %all-gather.3.cloned.1.call-update) | async-done | bytes 1048592 | tf_op jit(solution)/shard_map/all_gather | solution.py:19
  40.4 0.0 all-gather.5.cloned.1.call-update
  40.4 37.4 %all-to-all-done.1 = bf16[8,256,512]{2,1,0:T(8,128)(2,1)} async-done(((bf16[8,256,512]{2,1,0:T(8,128)(2,1)}), bf16[8,256,512]{2,1,0:T(8,128)(2,1)}, u32[]{:S(2)}, u32[]{:S(2)}) %all-to-all-start.1) | async-done | bytes 2097184 | tf_op jit(solution)/shard_map/all_to_all | solution.py:27
  77.8 0.0 copy-start.1
  77.8 0.0 copy-start.2
  77.8 4.5 %all-to-all-start = ((bf16[8,256,512]{2,1,0:T(8,128)(2,1)}), bf16[8,256,512]{2,1,0:T(8,128)(2,1)}, u32[]{:S(2)}, u32[]{:S(2)}) async-start(bf16[8,256,512]{2,1,0:T(8,128)(2,1)} %get-tuple-element.4), calls=%async_computation | async-start | bytes 4194304 | tf_op jit(solution)/shard_map/all_to_all | solution.py:27
  82.3 0.0 reduce-scatter.3.cloned.1.call-start
  82.4 0.0 copy-done.1
  82.4 0.0 copy-done.2
  82.4 55.0 %all_gather.11 = f32[1024,8]{0,1:T(8,128)S(1)} all-gather(f32[128,8]{0,1:T(8,128)S(1)} %select_reduce_fusion), channel_id=1, replica_groups=mesh['fs'=8,'tp'=4] {'fs'}, dimensions={0}, use_global_device_ids=true | all-gather | bytes 36864 | tf_op jit(solution)/shard_map/all_gather | solution.py:23
  137.4 0.0 all-gather.5.cloned.1.call-done
  137.5 6.5 %fusion.5 = f32[1024,512]{1,0:T(8,128)} fusion(bf16[1024,2048]{1,0:T(8,128)(2,1)} %all-gather.5.cloned.1.call-done, bf16[2048,512]{1,0:T(8,128)(2,1)} %bitcast.3), kind=kOutput, calls=%fused_computation.13 | convolution fusion | flops 2147483648 | bytes 8388608 | tf_op jit(solution)/shard_map/dot_general | solution.py:33
  144.0 0.0 all-to-all-done
  144.0 0.0 copy-done
  144.0 10.3 %multiply_convert_fusion = bf16[1024,2048]{1,0:T(8,128)(2,1)} fusion(f32[1024]{0:T(1024)S(1)} %bitcast.12, bf16[1,2048,512]{2,1,0:T(8,128)(2,1)S(1)} %copy-done, f32[1024,512]{1,0:T(8,128)} %fusion.5, bf16[1024,2048]{1,0:T(8,128)(2,1)} %all-gather.5.cloned.1.call-done, bf16[2048,512]{1,0:T(8,128)(2,1)} %bitcast.2), kind=kOutput, calls=%fused_computation | convolution fusion | flops 4304404480 | bytes 14684160 | tf_op jit(solution)/shard_map/dot_general | solution.py:40
  154.3 0.0 reduce-scatter.3.cloned.1.call-update
  154.3 0.0 reduce-scatter.5.cloned.1.call-start
  154.4 52.8 %reduce-scatter.3.cloned.1.call-done = bf16[1024,512]{1,0:T(8,128)(2,1)} async-done(((bf16[1024,2048]{1,0:T(8,128)(2,1)}), bf16[1024,512]{1,0:T(8,128)(2,1)}) %reduce-scatter.3.cloned.1.call-update) | async-done | bytes 1048592 | tf_op jit(solution)/shard_map/reduce_scatter | solution.py:44
  207.2 0.0 reduce-scatter.5.cloned.1.call-update
  207.2 35.4 %reduce-scatter.5.cloned.1.call-done = bf16[128,512]{1,0:T(8,128)(2,1)} async-done(((bf16[1024,512]{1,0:T(8,128)(2,1)}), bf16[128,512]{1,0:T(8,128)(2,1)}) %reduce-scatter.5.cloned.1.call-update) | async-done | bytes 131088 | tf_op jit(solution)/shard_map/reduce_scatter | solution.py:45
  242.6 3.0 %copy.16 = bf16[1,2048,512]{2,1,0:T(8,128)(2,1)} copy(bf16[1,2048,512]{2,1,0:T(8,128)(2,1)} %bitcast) | data formatting | bytes 4194304
  245.6 3.0 %copy.17 = bf16[1,2048,512]{2,1,0:T(8,128)(2,1)} copy(bf16[1,2048,512]{2,1,0:T(8,128)(2,1)} %bitcast.1) | data formatting | bytes 4194304
  (2 shorter events, 0.0 us)
Async XLA Ops:
  7.2 136.8 %copy-start = (bf16[1,2048,512]{2,1,0:T(8,128)(2,1)S(1)}, bf16[1,2048,512]{2,1,0:T(8,128)(2,1)}, u32[]{:S(2)}) copy-start(bf16[1,2048,512]{2,1,0:T(8,128)(2,1)} %param.13) | copy-start | bytes 6291460
  7.2 33.2 %all-gather.3.cloned.1.call-start = ((), (), s32[]{:S(2)}) async-start(), calls=%async_computation.4 | async-start | bytes 1179648 | tf_op jit(solution)/shard_map/all_gather | solution.py:19
  16.5 61.3 %all-to-all-start.1 = ((bf16[8,256,512]{2,1,0:T(8,128)(2,1)}), bf16[8,256,512]{2,1,0:T(8,128)(2,1)}, u32[]{:S(2)}, u32[]{:S(2)}) async-start(bf16[8,256,512]{2,1,0:T(8,128)(2,1)} %get-tuple-element.3), calls=%async_computation.1 | async-start | bytes 4194304 | tf_op jit(solution)/shard_map/all_to_all | solution.py:27
  22.9 114.6 %all-gather.5.cloned.1.call-start = ((), (), s32[]{:S(2)}) async-start(), calls=%async_computation.5 | async-start | bytes 5242880 | tf_op jit(solution)/shard_map/all_gather | solution.py:20
  77.8 4.6 %copy-start.1 = (f32[128,4]{0,1:T(4,128)S(1)}, f32[128,4]{0,1:T(4,128)}, u32[]{:S(2)}) copy-start(f32[128,4]{0,1:T(4,128)} %param.9) | copy-start | bytes 6148
  77.8 4.6 %copy-start.2 = (s32[128,4]{0,1:T(4,128)S(1)}, s32[128,4]{0,1:T(4,128)}, u32[]{:S(2)}) copy-start(s32[128,4]{0,1:T(4,128)} %param.8) | copy-start | bytes 6148
  77.8 66.2 %all-to-all-start = ((bf16[8,256,512]{2,1,0:T(8,128)(2,1)}), bf16[8,256,512]{2,1,0:T(8,128)(2,1)}, u32[]{:S(2)}, u32[]{:S(2)}) async-start(bf16[8,256,512]{2,1,0:T(8,128)(2,1)} %get-tuple-element.4), calls=%async_computation | async-start | bytes 4194304 | tf_op jit(solution)/shard_map/all_to_all | solution.py:27
  82.3 124.9 %reduce-scatter.3.cloned.1.call-start = ((), (), s32[]{:S(2)}) async-start(), calls=%async_computation.6 | async-start | bytes 5242880 | tf_op jit(solution)/shard_map/reduce_scatter | solution.py:44
  154.3 88.3 %reduce-scatter.5.cloned.1.call-start = ((), (), s32[]{:S(2)}) async-start(), calls=%async_computation.7 | async-start | bytes 1179648 | tf_op jit(solution)/shard_map/reduce_scatter | solution.py:45
Sparse Core Ops, SparseCore 0:
  10.2 30.2 all-gather.2
  42.2 56.2 all-gather.4
  154.4 52.7 reduce-scatter.2
  209.9 32.6 reduce-scatter.4

commit v2 on v1

v2 whole, which is shorter than its diff:
```python
import functools

import jax
import jax.numpy as jnp
from jax import lax
from jax.experimental import pallas as pl
from jax.experimental.pallas import tpu as pltpu
from jax.sharding import PartitionSpec as P

clamp_limit = 7.0
gate_slope = 1.702
CORES = 2
LANES = 128
MESH = pl.DeviceIdType.MESH
F32, BF16 = jnp.float32, jnp.bfloat16


def loop(lo, hi, body):
    if hi - lo <= 8:
        for k in range(lo, hi):
            body(k)
    else:
        lax.fori_loop(lo, hi, lambda k, c: (body(k), c)[1], 0)


def kernel(
    n_fs, n_tp, n_chunks,
    tokens_ref, share_ref, gain_ref, gate_ref, linear_ref, down_ref,
    gate_out, linear_out, mix_out,
    toks, stage_g, stage_l, wsend, wrecv, dts, acts, acc, shares,
    osend, orecv, zsend, zrecv,
    local_sem, stage_sem, own_sem, out_sem, dl_sem,
    w_s, w_r, s_s, s_r, t1_s, t1_r, t2_s, t2_r, t3_s, t3_r,
    d_s, d_r, a_s, a_r, o_s, o_r, z_s, z_r,
):
    fs, tp = lax.axis_index("fs"), lax.axis_index("tp")
    n_z = n_fs // CORES
    z, core = fs // CORES, lax.rem(fs, CORES)
    partner = z * CORES + (1 - core)
    tok, width = tokens_ref.shape
    experts, depth, cols = gate_ref.shape
    qcols = width // n_tp
    dcols = width // n_tp
    ch = cols // n_chunks

    def ds(i, n):
        return pl.ds(pl.multiple_of(i * n, n), n)

    def remote(src, dst, ss, rs, where):
        return pltpu.make_async_remote_copy(
            src_ref=src, dst_ref=dst, send_sem=ss, recv_sem=rs,
            device_id=where, device_id_type=MESH,
        )

    def peer_fs(k):
        return {"fs": lax.rem(fs + k, n_fs), "tp": tp}

    def peer_z(k):
        return {"fs": lax.rem(z + k, n_z) * CORES + core, "tp": tp}

    def peer_tp(k):
        return {"fs": fs, "tp": lax.rem(tp + k, n_tp)}

    over = {"fs": partner, "tp": tp}

    def stage(j):
        slot = j % 2
        c = pl.ds(j * ch, ch)
        return (
            pltpu.make_async_copy(gate_ref.at[:, :, c], stage_g.at[slot], stage_sem.at[0, slot]),
            pltpu.make_async_copy(linear_ref.at[:, :, c], stage_l.at[slot], stage_sem.at[1, slot]),
        )

    def src_fs(kz):
        return lax.rem(z + n_z - kz, n_z) * CORES + core

    def w_copy(j, k):
        to = lax.rem(fs + k, n_fs)
        return remote(wsend.at[j, to], wrecv.at[j, ds(fs, depth)], w_s.at[j, k], w_r.at[j, k], peer_fs(k))

    def w_own(j):
        return pltpu.make_async_copy(wsend.at[j, fs], wrecv.at[j, ds(fs, depth)], own_sem.at[j])

    def s_copy(k):
        return remote(share_ref, shares.at[fs], s_s.at[k], s_r.at[k], peer_fs(k))

    def t1_copy(k):
        block = toks.at[ds(fs, tok), ds(tp, qcols)]
        return remote(block, block, t1_s.at[k], t1_r.at[k], peer_z(k))

    def t2_copy(kz, k):
        block = toks.at[ds(src_fs(kz), tok), ds(tp, qcols)]
        return remote(block, block, t2_s.at[kz, k], t2_r.at[kz, k], peer_tp(k))

    def t3_copy(kz):
        block = toks.at[ds(src_fs(kz), tok)]
        return remote(block, block, t3_s.at[kz], t3_r.at[kz], over)

    def d_copy(j, k):
        to = lax.rem(tp + k, n_tp)
        return remote(
            down_ref.at[0, ds(to, dcols), pl.ds(j * ch, ch)],
            dts.at[j, :, ds(tp, ch)], d_s.at[j, k], d_r.at[j, k], peer_tp(k),
        )

    def d_own(j):
        return pltpu.make_async_copy(
            down_ref.at[0, ds(tp, dcols), pl.ds(j * ch, ch)], dts.at[j, :, ds(tp, ch)], dl_sem.at[j]
        )

    def a_copy(j, k):
        block = acts.at[j, :, ds(tp, ch)]
        return remote(block, block, a_s.at[j, k], a_r.at[j, k], peer_tp(k))

    def outs(j):
        c = pl.ds(j * ch, ch)
        return (
            pltpu.make_async_copy(wrecv.at[j, :, pl.ds(0, ch)], gate_out.at[0, :, c], out_sem.at[0, j]),
            pltpu.make_async_copy(wrecv.at[j, :, pl.ds(ch, ch)], linear_out.at[0, :, c], out_sem.at[1, j]),
        )

    def o_copy(kz):
        return remote(osend.at[kz], orecv.at[kz], o_s.at[kz], o_r.at[kz], over)

    def z_copy(kz):
        return remote(zsend.at[kz], zrecv.at[kz], z_s.at[kz], z_r.at[kz], peer_z(kz))

    own_tokens = pltpu.make_async_copy(tokens_ref, toks.at[ds(fs, tok)], local_sem.at[0])
    own_share = pltpu.make_async_copy(share_ref, shares.at[fs], local_sem.at[1])
    for c in (own_tokens, own_share, *stage(0)):
        c.start()

    barrier = pltpu.get_barrier_semaphore()
    loop(1, n_fs, lambda k: pl.semaphore_signal(barrier, inc=1, device_id=peer_fs(k), device_id_type=MESH))
    loop(1, n_tp, lambda k: pl.semaphore_signal(barrier, inc=1, device_id=peer_tp(k), device_id_type=MESH))
    pl.semaphore_wait(barrier, n_fs + n_tp - 2)

    own_tokens.wait()
    loop(1, n_z, lambda k: t1_copy(k).start())
    loop(1, n_fs, lambda k: s_copy(k).start())
    early = (n_chunks + 1) // 2
    for j in range(early):
        d_own(j).start()
        loop(1, n_tp, lambda k: d_copy(j, k).start())

    half = n_fs // 2
    for j in range(n_chunks):
        for c in stage(j):
            c.wait()
        if j + 1 < n_chunks:
            for c in stage(j + 1):
                c.start()

        def cast(e, carry):
            wsend[j, e, :, 0:ch] = (stage_g[j % 2, e] * gain_ref[...]).astype(BF16)
            wsend[j, e, :, ch:] = (stage_l[j % 2, e] * gain_ref[...]).astype(BF16)
            return carry

        lax.fori_loop(0, experts, cast, 0)
        loop(0, half, lambda i: w_copy(j, half - i).start())
        loop(half + 1, n_fs, lambda k: w_copy(j, k).start())
        w_own(j).start()

    def spread(kz):
        if not (isinstance(kz, int) and kz == 0):
            t1_copy(kz).wait_recv()
        loop(1, n_tp, lambda k: t2_copy(kz, k).start())

    loop(1, n_z, spread)
    for j in range(early, n_chunks):
        d_own(j).start()
        loop(1, n_tp, lambda k: d_copy(j, k).start())
    t3_copy(0).start()

    def join(kz):
        loop(1, n_tp, lambda k: t2_copy(kz, k).wait_recv())
        t3_copy(kz).start()

    loop(1, n_z, join)
    loop(0, n_z, lambda kz: t3_copy(kz).wait_recv())

    total = n_fs * tok
    rows = min(total, 256)

    def down(j):
        d_own(j).wait()
        loop(1, n_tp, lambda k: d_copy(j, k).wait_recv())
        loop(1, n_tp, lambda k: a_copy(j, k).wait_recv())

    def product(j, r):
        return lax.dot_general(
            acts[j, r, :], dts[j], (((1,), (1,)), ((), ())), preferred_element_type=F32
        )

    def accumulate(j):
        down(j)

        def step(i, carry):
            r = ds(i, rows)
            if j == 0:
                acc[r, :] = product(j, r)
            else:
                acc[r, :] += product(j, r)
            return carry

        lax.fori_loop(0, total // rows, step, 0)

    for j in range(n_chunks):
        w_own(j).wait()
        loop(1, n_fs, lambda k: w_copy(j, k).wait_recv())
        for c in outs(j):
            c.start()

        def up(i, carry):
            r = ds(i, rows)
            pre = jnp.dot(toks[r, :], wrecv[j], preferred_element_type=F32)
            c = jnp.minimum(pre[:, 0:ch], clamp_limit)
            lin = jnp.clip(pre[:, ch:], -clamp_limit, clamp_limit) + 1.0
            acts[j, r, ds(tp, ch)] = (c * jax.nn.sigmoid(gate_slope * c) * lin).astype(BF16)
            return carry

        lax.fori_loop(0, total // rows, up, 0)
        loop(1, n_tp, lambda k: a_copy(j, k).start())
        if j > 0:
            accumulate(j - 1)

    own_share.wait()
    loop(1, n_fs, lambda k: s_copy(k).wait_recv())
    last = n_chunks - 1
    down(last)

    def weighted(who):
        r = ds(who, tok)
        value = product(last, r)
        if last > 0:
            value = value + acc[r, :]
        line = shares[who, pl.ds(fs, 1), :]
        w = jnp.transpose(jnp.broadcast_to(line, (tok, tok)))
        return value * jnp.concatenate([w] * (dcols // LANES), axis=1)

    def give(kz):
        to = lax.rem(z + kz, n_z) * CORES + (1 - core)
        osend[kz] = weighted(to).astype(BF16)
        o_copy(kz).start()

    def keep(kz):
        to = lax.rem(z + kz, n_z) * CORES + core
        acc[ds(to, tok), :] = weighted(to)

    def pass_on(kz):
        to = lax.rem(z + kz, n_z) * CORES + core
        o_copy(kz).wait_recv()
        zsend[kz] = (acc[ds(to, tok), :] + orecv[kz].astype(F32)).astype(BF16)
        z_copy(kz).start()

    loop(1, n_z, give)
    give(0)
    loop(1, n_z, keep)
    keep(0)
    loop(1, n_z, pass_on)
    o_copy(0).wait_recv()
    r = ds(fs, tok)
    acc[r, :] += orecv[0].astype(F32)

    def gather(kz):
        z_copy(kz).wait_recv()
        acc[r, :] += zrecv[kz].astype(F32)

    loop(1, n_z, gather)
    mix_out[...] = acc[r, :].astype(BF16)

    for j in range(n_chunks):
        for c in outs(j):
            c.wait()
        loop(1, n_fs, lambda k: w_copy(j, k).wait_send())
        loop(1, n_tp, lambda k: d_copy(j, k).wait_send())
        loop(1, n_tp, lambda k: a_copy(j, k).wait_send())
    loop(1, n_fs, lambda k: s_copy(k).wait_send())
    loop(1, n_z, lambda k: t1_copy(k).wait_send())
    loop(1, n_z, lambda kz: loop(1, n_tp, lambda k: t2_copy(kz, k).wait_send()))
    loop(0, n_z, lambda kz: t3_copy(kz).wait_send())
    loop(0, n_z, lambda kz: o_copy(kz).wait_send())
    loop(1, n_z, lambda kz: z_copy(kz).wait_send())


def solution(mesh):
    n_fs, n_tp = mesh.shape["fs"], mesh.shape["tp"]

    def on_device(tokens, experts, routing, norm_gain, gate_master, linear_master, down_weight):
        expert_count, depth, cols = gate_master.shape
        tok, width = tokens.shape
        n_z = n_fs // CORES
        ch = min(LANES, cols)
        n_chunks = cols // ch
        dcols = width // n_tp
        fs = lax.axis_index("fs")
        choice = experts.T[:, None, :] == jnp.arange(expert_count, dtype=jnp.int32)[None, :, None]
        share = jnp.sum(jnp.where(choice, routing.T[:, None, :], 0.0), axis=0)
        gain = lax.dynamic_slice_in_dim(norm_gain, fs * depth, depth, axis=0)
        gain = jnp.broadcast_to(gain[:, None], (depth, ch))
        hbm = pl.BlockSpec(memory_space=pl.ANY)
        vmem = pl.BlockSpec(memory_space=pltpu.VMEM)
        dma = pltpu.SemaphoreType.DMA
        slots = min(2, n_chunks)
        out_shape = jax.ShapeDtypeStruct((1, width, cols), BF16)
        pairs = [
            (n_chunks, n_fs), (n_fs,), (n_z,), (n_z, n_tp), (n_z,),
            (n_chunks, n_tp), (n_chunks, n_tp), (n_z,), (n_z,),
        ]
        return pl.pallas_call(
            functools.partial(kernel, n_fs, n_tp, n_chunks),
            out_shape=(out_shape, out_shape, jax.ShapeDtypeStruct((tok, dcols), BF16)),
            in_specs=[hbm, vmem, vmem, hbm, hbm, hbm],
            out_specs=(hbm, hbm, vmem),
            scratch_shapes=[
                pltpu.VMEM((n_fs * tok, width), BF16),
                pltpu.VMEM((slots, expert_count, depth, ch), F32),
                pltpu.VMEM((slots, expert_count, depth, ch), F32),
                pltpu.VMEM((n_chunks, expert_count, depth, 2 * ch), BF16),
                pltpu.VMEM((n_chunks, width, 2 * ch), BF16),
                pltpu.VMEM((n_chunks, dcols, n_tp * ch), BF16),
                pltpu.VMEM((n_chunks, n_fs * tok, n_tp * ch), BF16),
                pltpu.VMEM((n_fs * tok, dcols), F32),
                pltpu.VMEM((n_fs, expert_count, tok), F32),
                pltpu.VMEM((n_z, tok, dcols), BF16),
                pltpu.VMEM((n_z, tok, dcols), BF16),
                pltpu.VMEM((n_z, tok, dcols), BF16),
                pltpu.VMEM((n_z, tok, dcols), BF16),
                dma((2,)), dma((2, slots)), dma((n_chunks,)), dma((2, n_chunks)), dma((n_chunks,)),
            ] + [dma(shape) for shape in pairs for _ in range(2)],
            compiler_params=pltpu.CompilerParams(collective_id=0, has_side_effects=True),
        )(tokens, share, gain, gate_master, linear_master, down_weight)

    placed = (
        P("fs", None),
        P("fs", None),
        P("fs", None),
        P(),
        P(None, "fs", "tp"),
        P(None, "fs", "tp"),
        P("fs", None, "tp"),
    )
    return jax.shard_map(
        on_device,
        mesh=mesh,
        in_specs=placed,
        out_specs=(P("fs", None, "tp"), P("fs", None, "tp"), P("fs", "tp")),
        check_vma=False,
    )
```

time: 256 us -> 147 us (0.57)
  waiting for transfers between devices: 143 us -> 0 us
  Pallas kernels: 0 us -> 136 us
  blocking collectives: 55 us -> 0 us
  matrix products: 16.8 us -> 0 us
  between operations: 13.8 us -> 0.65 us
  starting transfers between devices: 11 us -> 0 us
  other arithmetic: 6.81 us -> 1.3 us
    pallas_call x0 -> x1, Pallas kernels: none -> 136 us  [on_device(): pl.pallas_call(functools.partial(kernel, n_fs, n_tp, n_chunks), out_shape...]
    reduce_scatter x2 -> x0, waiting for transfers between devices: 88.2 us -> none  [the longest x1 52.8 us: on_device(): summed = lax.psum_scatter(part, 'tp', scatter_dimension=1, tiled=True)]
    all_gather x1 -> x0, blocking collectives: 55 us -> none  [on_device(): shares = lax.all_gather(share, 'fs', axis=0, tiled=True)]
    all_to_all x2 -> x0, waiting for transfers between devices: 37.4 us -> none  [on_device(): lax.all_to_all((master * gain).astype(jnp.bfloat16), 'fs', split_axis=0,...]
    all_gather x2 -> x0, waiting for transfers between devices: 17.5 us -> none  [the longest x1 17.5 us: on_device(): quarter = lax.all_gather(mine, 'fs', axis=0, tiled=True)]
    dot_general x2 -> x0, matrix products: 16.8 us -> none  [the longest x1 10.3 us: on_device(): lax.dot_general(active, down_weight[0], (((1,), (1,)), ((), ())), preferr...]
    all_to_all x2 -> x0, starting transfers between devices: 10.8 us -> none  [on_device(): lax.all_to_all((master * gain).astype(jnp.bfloat16), 'fs', split_axis=0,...]
    convert_element_type x1 -> x0, other arithmetic: 6.8 us -> none  [on_device(): (master * gain).astype(jnp.bfloat16)]
  transfers between devices with their start and end apart: 6 -> 0, of which waited for: 4 -> 0; matrix products, arithmetic and copies ran while one was open for 6% -> 0% of each run, Pallas kernels for 0% -> 0%
where the time goes in v2:
time: 147 us; the launch traced here: 145 us
  Pallas kernels  136 us (93%)
  local copies, waits for them, and re-layouts  6.69 us (5%)
    pallas_call x1, Pallas kernels, on_device(): pl.pallas_call(functools.partial(kernel, n_fs, n_tp, n_chunks), out_shape...  136 us
    unnamed x7, local copies, waits for them, and re-layouts  5.18 us

profile of v2, /device:TPU:0, one launch (start us, length us, event | category | flops | bytes accessed | tf_op | source)
XLA Modules:
  0.0 144.9 jit_solution(5716592851013765171)
XLA Ops:
  0.6 0.8 dynamic_slice.3
  1.4 1.3 select_reduce_fusion.share_ref
  2.7 0.8 broadcast_in_dim.23.gain_ref
  3.5 136.2 %shard_map.94 = (bf16[1,2048,512]{2,1,0:T(8,128)(2,1)}, bf16[1,2048,512]{2,1,0:T(8,128)(2,1)}, bf16[128,512]{1,0:T(8,128)(2,1)}) custom-call(bf16[128,2048]{1,0:T(8,128)(2,1)} %tokens_ref.1, f32[8,128]{1,0:T(8,128)} %select_reduce_fusion.share_ref, f32[256,128]{1,0:T(8,128)} %broadcast_in_dim.23.gain_ref, f32[8,256,512]{2,1,0:T(8,128)} %gate_ref.1, ...), custom_call_target="tpu_custom_call" | custom-call | tf_op jit(solution)/shard_map/pallas_call | solution.py:310
  139.7 0.0 copy-start
  139.7 3.2 %copy.13 = bf16[1,2048,512]{2,1,0:T(8,128)(2,1)} copy(bf16[1,2048,512]{2,1,0:T(8,128)(2,1)} %get-tuple-element.6) | data formatting | bytes 4194304
  142.9 0.0 copy-done
  142.9 0.0 copy-start.1
  142.9 1.3 copy.14
  144.2 0.0 copy-done.1
  144.2 0.7 copy.15
Async XLA Ops:
  139.7 3.2 %copy-start = (bf16[1,2048,512]{2,1,0:T(8,128)(2,1)S(1)}, bf16[1,2048,512]{2,1,0:T(8,128)(2,1)}, u32[]{:S(2)}) copy-start(bf16[1,2048,512]{2,1,0:T(8,128)(2,1)} %get-tuple-element.7) | copy-start | bytes 6291460
  142.9 1.3 copy-start.1

commit v3 on v2

--- a/solution.py
+++ b/solution.py
@@ -25,13 +25,13 @@
 
 def kernel(
     n_fs, n_tp, n_chunks,
-    tokens_ref, share_ref, gain_ref, gate_ref, linear_ref, down_ref,
+    tokens_ref, experts_ref, routing_ref, gain_ref, gate_ref, linear_ref, down_ref,
     gate_out, linear_out, mix_out,
-    toks, stage_g, stage_l, wsend, wrecv, dts, acts, acc, shares,
+    toks, gains, stage_g, stage_l, wsend, wrecv, dts, acts, acc, shares,
     osend, orecv, zsend, zrecv,
     local_sem, stage_sem, own_sem, out_sem, dl_sem,
     w_s, w_r, s_s, s_r, t1_s, t1_r, t2_s, t2_r, t3_s, t3_r,
-    d_s, d_r, a_s, a_r, o_s, o_r, z_s, z_r,
+    d_s, d_r, a_s, a_r, l_s, l_r, o_s, o_r, z_s, z_r,
 ):
     fs, tp = lax.axis_index("fs"), lax.axis_index("tp")
     n_z = n_fs // CORES
@@ -82,7 +82,7 @@
         return pltpu.make_async_copy(wsend.at[j, fs], wrecv.at[j, ds(fs, depth)], own_sem.at[j])
 
     def s_copy(k):
-        return remote(share_ref, shares.at[fs], s_s.at[k], s_r.at[k], peer_fs(k))
+        return remote(shares.at[fs], shares.at[fs], s_s.at[k], s_r.at[k], peer_fs(k))
 
     def t1_copy(k):
         block = toks.at[ds(fs, tok), ds(tp, qcols)]
@@ -122,27 +122,49 @@
     def o_copy(kz):
         return remote(osend.at[kz], orecv.at[kz], o_s.at[kz], o_r.at[kz], over)
 
-    def z_copy(kz):
-        return remote(zsend.at[kz], zrecv.at[kz], z_s.at[kz], z_r.at[kz], peer_z(kz))
+    def zx(m):
+        out, bit = z, 1
+        while bit <= m:
+            if m & bit:
+                out = out + bit - 2 * bit * lax.rem(z // bit, 2)
+            bit *= 2
+        return out
+
+    def l_copy(m, k):
+        block = acts.at[n_chunks - 1, ds(zx(m), CORES * tok), ds(tp, ch)]
+        return remote(block, block, l_s.at[m, k], l_r.at[m, k], peer_tp(k))
+
+    def z_copy(m):
+        where = {"fs": zx(m) * CORES + core, "tp": tp}
+        return remote(zsend.at[m], zrecv.at[m], z_s.at[m], z_r.at[m], where)
 
     own_tokens = pltpu.make_async_copy(tokens_ref, toks.at[ds(fs, tok)], local_sem.at[0])
-    own_share = pltpu.make_async_copy(share_ref, shares.at[fs], local_sem.at[1])
-    for c in (own_tokens, own_share, *stage(0)):
+    for c in (own_tokens, *stage(0)):
         c.start()
 
     barrier = pltpu.get_barrier_semaphore()
     loop(1, n_fs, lambda k: pl.semaphore_signal(barrier, inc=1, device_id=peer_fs(k), device_id_type=MESH))
     loop(1, n_tp, lambda k: pl.semaphore_signal(barrier, inc=1, device_id=peer_tp(k), device_id_type=MESH))
+
+    lane = lax.broadcasted_iota(jnp.int32, (tok, LANES), 1)
+    share = jnp.zeros((tok, LANES), F32)
+    for k in range(experts_ref.shape[1]):
+        share += jnp.where(experts_ref[:, k : k + 1] == lane, routing_ref[:, k : k + 1], 0.0)
+    shares[fs] = jnp.transpose(share)[:experts]
+    for i in range(max(depth // LANES, 1)):
+        line = gain_ref[pl.ds(fs * depth // LANES + i, 1), :]
+        gains[i * LANES : (i + 1) * LANES, :] = jnp.transpose(jnp.broadcast_to(line, (LANES, LANES)))
+    gain_rows = pl.ds(pl.multiple_of(lax.rem(fs * depth, LANES), 8), depth)
     pl.semaphore_wait(barrier, n_fs + n_tp - 2)
 
     own_tokens.wait()
     loop(1, n_z, lambda k: t1_copy(k).start())
-    loop(1, n_fs, lambda k: s_copy(k).start())
     early = (n_chunks + 1) // 2
     for j in range(early):
         d_own(j).start()
         loop(1, n_tp, lambda k: d_copy(j, k).start())
 
+    loop(1, n_fs, lambda k: s_copy(k).start())
     half = n_fs // 2
     for j in range(n_chunks):
         for c in stage(j):
@@ -152,8 +174,8 @@
                 c.start()
 
         def cast(e, carry):
-            wsend[j, e, :, 0:ch] = (stage_g[j % 2, e] * gain_ref[...]).astype(BF16)
-            wsend[j, e, :, ch:] = (stage_l[j % 2, e] * gain_ref[...]).astype(BF16)
+            wsend[j, e, :, 0:ch] = (stage_g[j % 2, e] * gains[gain_rows, 0:ch]).astype(BF16)
+            wsend[j, e, :, ch:] = (stage_l[j % 2, e] * gains[gain_rows, 0:ch]).astype(BF16)
             return carry
 
         lax.fori_loop(0, experts, cast, 0)
@@ -185,7 +207,8 @@
     def down(j):
         d_own(j).wait()
         loop(1, n_tp, lambda k: d_copy(j, k).wait_recv())
-        loop(1, n_tp, lambda k: a_copy(j, k).wait_recv())
+        if j < n_chunks - 1:
+            loop(1, n_tp, lambda k: a_copy(j, k).wait_recv())
 
     def product(j, r):
         return lax.dot_general(
@@ -205,28 +228,29 @@
 
         lax.fori_loop(0, total // rows, step, 0)
 
-    for j in range(n_chunks):
+    def arrive(j):
         w_own(j).wait()
         loop(1, n_fs, lambda k: w_copy(j, k).wait_recv())
         for c in outs(j):
             c.start()
 
-        def up(i, carry):
-            r = ds(i, rows)
-            pre = jnp.dot(toks[r, :], wrecv[j], preferred_element_type=F32)
-            c = jnp.minimum(pre[:, 0:ch], clamp_limit)
-            lin = jnp.clip(pre[:, ch:], -clamp_limit, clamp_limit) + 1.0
-            acts[j, r, ds(tp, ch)] = (c * jax.nn.sigmoid(gate_slope * c) * lin).astype(BF16)
-            return carry
-
-        lax.fori_loop(0, total // rows, up, 0)
+    def up(j, r):
+        pre = jnp.dot(toks[r, :], wrecv[j], preferred_element_type=F32)
+        c = jnp.minimum(pre[:, 0:ch], clamp_limit)
+        lin = jnp.clip(pre[:, ch:], -clamp_limit, clamp_limit) + 1.0
+        acts[j, r, ds(tp, ch)] = (c * jax.nn.sigmoid(gate_slope * c) * lin).astype(BF16)
+
+    last = n_chunks - 1
+    for j in range(last):
+        arrive(j)
+        lax.fori_loop(0, total // rows, lambda i, c: (up(j, ds(i, rows)), c)[1], 0)
         loop(1, n_tp, lambda k: a_copy(j, k).start())
         if j > 0:
             accumulate(j - 1)
-
-    own_share.wait()
+    if last > 0:
+        accumulate(last - 1)
+
     loop(1, n_fs, lambda k: s_copy(k).wait_recv())
-    last = n_chunks - 1
     down(last)
 
     def weighted(who):
@@ -238,35 +262,33 @@
         w = jnp.transpose(jnp.broadcast_to(line, (tok, tok)))
         return value * jnp.concatenate([w] * (dcols // LANES), axis=1)
 
-    def give(kz):
-        to = lax.rem(z + kz, n_z) * CORES + (1 - core)
-        osend[kz] = weighted(to).astype(BF16)
-        o_copy(kz).start()
-
-    def keep(kz):
-        to = lax.rem(z + kz, n_z) * CORES + core
-        acc[ds(to, tok), :] = weighted(to)
-
-    def pass_on(kz):
-        to = lax.rem(z + kz, n_z) * CORES + core
-        o_copy(kz).wait_recv()
-        zsend[kz] = (acc[ds(to, tok), :] + orecv[kz].astype(F32)).astype(BF16)
-        z_copy(kz).start()
-
-    loop(1, n_z, give)
-    give(0)
-    loop(1, n_z, keep)
-    keep(0)
-    loop(1, n_z, pass_on)
-    o_copy(0).wait_recv()
+    def pass_on(m):
+        r = ds(zx(m) * CORES + core, tok)
+        o_copy(m).wait_recv()
+        if m == 0:
+            acc[r, :] += orecv[m].astype(F32)
+        else:
+            zsend[m] = (acc[r, :] + orecv[m].astype(F32)).astype(BF16)
+            z_copy(m).start()
+
+    order = list(range(n_z - 1, -1, -1))
+    arrive(last)
+    for m in order:
+        up(last, ds(zx(m), CORES * tok))
+        loop(1, n_tp, lambda k: l_copy(m, k).start())
+    for m in order:
+        loop(1, n_tp, lambda k: l_copy(m, k).wait_recv())
+        osend[m] = weighted(zx(m) * CORES + (1 - core)).astype(BF16)
+        o_copy(m).start()
+        kept = zx(m) * CORES + core
+        acc[ds(kept, tok), :] = weighted(kept)
+        if m < n_z - 1:
+            pass_on(m + 1)
+    pass_on(0)
     r = ds(fs, tok)
-    acc[r, :] += orecv[0].astype(F32)
-
-    def gather(kz):
-        z_copy(kz).wait_recv()
-        acc[r, :] += zrecv[kz].astype(F32)
-
-    loop(1, n_z, gather)
+    for m in order[:-1]:
+        z_copy(m).wait_recv()
+        acc[r, :] += zrecv[m].astype(F32)
     mix_out[...] = acc[r, :].astype(BF16)
 
     for j in range(n_chunks):
@@ -274,13 +296,17 @@
             c.wait()
         loop(1, n_fs, lambda k: w_copy(j, k).wait_send())
         loop(1, n_tp, lambda k: d_copy(j, k).wait_send())
-        loop(1, n_tp, lambda k: a_copy(j, k).wait_send())
+        if j < last:
+            loop(1, n_tp, lambda k: a_copy(j, k).wait_send())
+    for m in order:
+        loop(1, n_tp, lambda k: l_copy(m, k).wait_send())
     loop(1, n_fs, lambda k: s_copy(k).wait_send())
     loop(1, n_z, lambda k: t1_copy(k).wait_send())
     loop(1, n_z, lambda kz: loop(1, n_tp, lambda k: t2_copy(kz, k).wait_send()))
     loop(0, n_z, lambda kz: t3_copy(kz).wait_send())
     loop(0, n_z, lambda kz: o_copy(kz).wait_send())
-    loop(1, n_z, lambda kz: z_copy(kz).wait_send())
+    for m in order[:-1]:
+        z_copy(m).wait_send()
 
 
 def solution(mesh):
@@ -293,11 +319,7 @@
         ch = min(LANES, cols)
         n_chunks = cols // ch
         dcols = width // n_tp
-        fs = lax.axis_index("fs")
-        choice = experts.T[:, None, :] == jnp.arange(expert_count, dtype=jnp.int32)[None, :, None]
-        share = jnp.sum(jnp.where(choice, routing.T[:, None, :], 0.0), axis=0)
-        gain = lax.dynamic_slice_in_dim(norm_gain, fs * depth, depth, axis=0)
-        gain = jnp.broadcast_to(gain[:, None], (depth, ch))
+        lines = norm_gain.reshape(width // LANES, LANES)
         hbm = pl.BlockSpec(memory_space=pl.ANY)
         vmem = pl.BlockSpec(memory_space=pltpu.VMEM)
         dma = pltpu.SemaphoreType.DMA
@@ -305,15 +327,16 @@
         out_shape = jax.ShapeDtypeStruct((1, width, cols), BF16)
         pairs = [
             (n_chunks, n_fs), (n_fs,), (n_z,), (n_z, n_tp), (n_z,),
-            (n_chunks, n_tp), (n_chunks, n_tp), (n_z,), (n_z,),
+            (n_chunks, n_tp), (n_chunks, n_tp), (n_z, n_tp), (n_z,), (n_z,),
         ]
         return pl.pallas_call(
             functools.partial(kernel, n_fs, n_tp, n_chunks),
             out_shape=(out_shape, out_shape, jax.ShapeDtypeStruct((tok, dcols), BF16)),
-            in_specs=[hbm, vmem, vmem, hbm, hbm, hbm],
+            in_specs=[hbm, vmem, vmem, vmem, hbm, hbm, hbm],
             out_specs=(hbm, hbm, vmem),
             scratch_shapes=[
                 pltpu.VMEM((n_fs * tok, width), BF16),
+                pltpu.VMEM((max(depth, LANES), LANES), F32),
                 pltpu.VMEM((slots, expert_count, depth, ch), F32),
                 pltpu.VMEM((slots, expert_count, depth, ch), F32),
                 pltpu.VMEM((n_chunks, expert_count, depth, 2 * ch), BF16),
@@ -329,7 +352,7 @@
                 dma((2,)), dma((2, slots)), dma((n_chunks,)), dma((2, n_chunks)), dma((n_chunks,)),
             ] + [dma(shape) for shape in pairs for _ in range(2)],
             compiler_params=pltpu.CompilerParams(collective_id=0, has_side_effects=True),
-        )(tokens, share, gain, gate_master, linear_master, down_weight)
+        )(tokens, experts, routing, lines, gate_master, linear_master, down_weight)
 
     placed = (
         P("fs", None),

time: 147 us -> 147 us (level); the launches traced: 145 us -> 146 us
  Pallas kernels: 136 us -> 138 us
    unnamed x7 -> x9, local copies, waits for them, and re-layouts: 5.18 us -> 8.01 us
    pallas_call x1, Pallas kernels: 136 us -> 138 us  [on_device(): pl.pallas_call(functools.partial(kernel, n_fs, n_tp, n_chunks), out_shape...]
where the time goes in v3:
time: 147 us; the launch traced here: 146 us
  Pallas kernels  138 us (94%)
  local copies, waits for them, and re-layouts  8.01 us (5%)
    pallas_call x1, Pallas kernels, on_device(): pl.pallas_call(functools.partial(kernel, n_fs, n_tp, n_chunks), out_shape...  138 us
    unnamed x9, local copies, waits for them, and re-layouts  8.01 us

profile of v3, /device:TPU:0, one launch (start us, length us, event | category | flops | bytes accessed | tf_op | source)
XLA Modules:
  0.0 146.5 jit_solution(16998443926485991605)
XLA Ops:
  0.6 1.4 copy.10.experts_ref
  2.0 1.4 copy.11.routing_ref
  3.5 137.8 %shard_map.94 = (bf16[1,2048,512]{2,1,0:T(8,128)(2,1)}, bf16[1,2048,512]{2,1,0:T(8,128)(2,1)}, bf16[128,512]{1,0:T(8,128)(2,1)}) custom-call(bf16[128,2048]{1,0:T(8,128)(2,1)} %tokens_ref.1, s32[128,4]{1,0:T(8,128)} %copy.10.experts_ref, f32[128,4]{1,0:T(8,128)} %copy.11.routing_ref, f32[16,128]{1,0:T(8,128)} %bitcast.1, f32[8,256,512]{2,1,0:T(8,128)} %gate_ref.1, ...), custom_call_target="tpu_custom_call" | custom-call | tf_op jit(solution)/shard_map/pallas_call | solution.py:332
  141.3 0.0 copy-start
  141.3 3.2 %copy.15 = bf16[1,2048,512]{2,1,0:T(8,128)(2,1)} copy(bf16[1,2048,512]{2,1,0:T(8,128)(2,1)} %get-tuple-element.6) | data formatting | bytes 4194304
  144.5 0.0 copy-done
  144.5 0.0 copy-start.1
  144.5 1.3 copy.16
  145.8 0.0 copy-done.1
  145.8 0.7 copy.17
Async XLA Ops:
  141.3 3.2 %copy-start = (bf16[1,2048,512]{2,1,0:T(8,128)(2,1)S(1)}, bf16[1,2048,512]{2,1,0:T(8,128)(2,1)}, u32[]{:S(2)}) copy-start(bf16[1,2048,512]{2,1,0:T(8,128)(2,1)} %get-tuple-element.7) | copy-start | bytes 6291460
  144.5 1.3 copy-start.1

commit v4 on v3

--- a/solution.py
+++ b/solution.py
@@ -37,12 +37,24 @@
     n_z = n_fs // CORES
     z, core = fs // CORES, lax.rem(fs, CORES)
     partner = z * CORES + (1 - core)
+    across = n_z // 2
     tok, width = tokens_ref.shape
     experts, depth, cols = gate_ref.shape
     qcols = width // n_tp
     dcols = width // n_tp
     ch = cols // n_chunks
 
+    def flip(index, mask):
+        out, bit = index, 1
+        while bit <= mask:
+            if mask & bit:
+                out = out + bit - 2 * bit * lax.rem(index // bit, 2)
+            bit *= 2
+        return out
+
+    def zx(m):
+        return flip(z, m)
+
     def ds(i, n):
         return pl.ds(pl.multiple_of(i * n, n), n)
 
@@ -54,9 +66,6 @@
 
     def peer_fs(k):
         return {"fs": lax.rem(fs + k, n_fs), "tp": tp}
-
-    def peer_z(k):
-        return {"fs": lax.rem(z + k, n_z) * CORES + core, "tp": tp}
 
     def peer_tp(k):
         return {"fs": fs, "tp": lax.rem(tp + k, n_tp)}
@@ -71,12 +80,14 @@
             pltpu.make_async_copy(linear_ref.at[:, :, c], stage_l.at[slot], stage_sem.at[1, slot]),
         )
 
-    def src_fs(kz):
-        return lax.rem(z + n_z - kz, n_z) * CORES + core
+    def src_fs(m):
+        return zx(m) * CORES + core
 
     def w_copy(j, k):
-        to = lax.rem(fs + k, n_fs)
-        return remote(wsend.at[j, to], wrecv.at[j, ds(fs, depth)], w_s.at[j, k], w_r.at[j, k], peer_fs(k))
+        to = flip(fs, k)
+        return remote(
+            wsend.at[j, to], wrecv.at[j, ds(fs, depth)], w_s.at[j, k], w_r.at[j, k], {"fs": to, "tp": tp}
+        )
 
     def w_own(j):
         return pltpu.make_async_copy(wsend.at[j, fs], wrecv.at[j, ds(fs, depth)], own_sem.at[j])
@@ -84,9 +95,10 @@
     def s_copy(k):
         return remote(shares.at[fs], shares.at[fs], s_s.at[k], s_r.at[k], peer_fs(k))
 
-    def t1_copy(k):
-        block = toks.at[ds(fs, tok), ds(tp, qcols)]
-        return remote(block, block, t1_s.at[k], t1_r.at[k], peer_z(k))
+    def t1_copy(m):
+        block = toks.at[ds(fs if m <= across else src_fs(across), tok), ds(tp, qcols)]
+        to = m if m <= across else m - across
+        return remote(block, block, t1_s.at[m], t1_r.at[m], {"fs": src_fs(to), "tp": tp})
 
     def t2_copy(kz, k):
         block = toks.at[ds(src_fs(kz), tok), ds(tp, qcols)]
@@ -122,14 +134,6 @@
     def o_copy(kz):
         return remote(osend.at[kz], orecv.at[kz], o_s.at[kz], o_r.at[kz], over)
 
-    def zx(m):
-        out, bit = z, 1
-        while bit <= m:
-            if m & bit:
-                out = out + bit - 2 * bit * lax.rem(z // bit, 2)
-            bit *= 2
-        return out
-
     def l_copy(m, k):
         block = acts.at[n_chunks - 1, ds(zx(m), CORES * tok), ds(tp, ch)]
         return remote(block, block, l_s.at[m, k], l_r.at[m, k], peer_tp(k))
@@ -146,11 +150,11 @@
     loop(1, n_fs, lambda k: pl.semaphore_signal(barrier, inc=1, device_id=peer_fs(k), device_id_type=MESH))
     loop(1, n_tp, lambda k: pl.semaphore_signal(barrier, inc=1, device_id=peer_tp(k), device_id_type=MESH))
 
-    lane = lax.broadcasted_iota(jnp.int32, (tok, LANES), 1)
-    share = jnp.zeros((tok, LANES), F32)
-    for k in range(experts_ref.shape[1]):
-        share += jnp.where(experts_ref[:, k : k + 1] == lane, routing_ref[:, k : k + 1], 0.0)
-    shares[fs] = jnp.transpose(share)[:experts]
+    expert = lax.broadcasted_iota(jnp.int32, (experts, tok), 0)
+    share = jnp.zeros((experts, tok), F32)
+    for k in range(experts_ref.shape[0]):
+        share += jnp.where(experts_ref[k : k + 1, :] == expert, routing_ref[k : k + 1, :], 0.0)
+    shares[fs] = share
     for i in range(max(depth // LANES, 1)):
         line = gain_ref[pl.ds(fs * depth // LANES + i, 1), :]
         gains[i * LANES : (i + 1) * LANES, :] = jnp.transpose(jnp.broadcast_to(line, (LANES, LANES)))
@@ -158,7 +162,8 @@
     pl.semaphore_wait(barrier, n_fs + n_tp - 2)
 
     own_tokens.wait()
-    loop(1, n_z, lambda k: t1_copy(k).start())
+    for m in range(across, 0, -1):
+        t1_copy(m).start()
     early = (n_chunks + 1) // 2
     for j in range(early):
         d_own(j).start()
@@ -166,7 +171,8 @@
 
     loop(1, n_fs, lambda k: s_copy(k).start())
     half = n_fs // 2
-    for j in range(n_chunks):
+
+    def prepare(j):
         for c in stage(j):
             c.wait()
         if j + 1 < n_chunks:
@@ -179,27 +185,41 @@
             return carry
 
         lax.fori_loop(0, experts, cast, 0)
-        loop(0, half, lambda i: w_copy(j, half - i).start())
-        loop(half + 1, n_fs, lambda k: w_copy(j, k).start())
         w_own(j).start()
-
-    def spread(kz):
-        if not (isinstance(kz, int) and kz == 0):
-            t1_copy(kz).wait_recv()
-        loop(1, n_tp, lambda k: t2_copy(kz, k).start())
-
-    loop(1, n_z, spread)
+        for k in range(half - 1, 0, -1):
+            w_copy(j, k).start()
+
+    def spread(m):
+        t1_copy(m).wait_recv()
+        loop(1, n_tp, lambda k: t2_copy(m, k).start())
+
+    crossing = list(range(n_fs - 1, half - 1, -1))
+    prepare(0)
+    for k in crossing[: half // 2]:
+        w_copy(0, k).start()
+    spread(across)
+    for m in range(across + 1, n_z):
+        t1_copy(m).start()
+    for k in crossing[half // 2 :]:
+        w_copy(0, k).start()
+    t3_copy(0).start()
+    for m in range(1, across):
+        spread(m)
+    for j in range(1, n_chunks):
+        prepare(j)
+    for j in range(1, n_chunks):
+        for k in crossing:
+            w_copy(j, k).start()
+    for m in range(across + 1, n_z):
+        spread(m)
     for j in range(early, n_chunks):
         d_own(j).start()
         loop(1, n_tp, lambda k: d_copy(j, k).start())
-    t3_copy(0).start()
-
-    def join(kz):
-        loop(1, n_tp, lambda k: t2_copy(kz, k).wait_recv())
-        t3_copy(kz).start()
-
-    loop(1, n_z, join)
-    loop(0, n_z, lambda kz: t3_copy(kz).wait_recv())
+    for m in range(1, n_z):
+        loop(1, n_tp, lambda k: t2_copy(m, k).wait_recv())
+        t3_copy(m).start()
+    for m in range(n_z):
+        t3_copy(m).wait_recv()
 
     total = n_fs * tok
     rows = min(total, 256)
@@ -230,7 +250,8 @@
 
     def arrive(j):
         w_own(j).wait()
-        loop(1, n_fs, lambda k: w_copy(j, k).wait_recv())
+        for k in range(1, n_fs):
+            w_copy(j, k).wait_recv()
         for c in outs(j):
             c.start()
 
@@ -294,16 +315,19 @@
     for j in range(n_chunks):
         for c in outs(j):
             c.wait()
-        loop(1, n_fs, lambda k: w_copy(j, k).wait_send())
+        for k in range(1, n_fs):
+            w_copy(j, k).wait_send()
         loop(1, n_tp, lambda k: d_copy(j, k).wait_send())
         if j < last:
             loop(1, n_tp, lambda k: a_copy(j, k).wait_send())
     for m in order:
         loop(1, n_tp, lambda k: l_copy(m, k).wait_send())
     loop(1, n_fs, lambda k: s_copy(k).wait_send())
-    loop(1, n_z, lambda k: t1_copy(k).wait_send())
-    loop(1, n_z, lambda kz: loop(1, n_tp, lambda k: t2_copy(kz, k).wait_send()))
-    loop(0, n_z, lambda kz: t3_copy(kz).wait_send())
+    for m in range(n_z):
+        if m > 0:
+            t1_copy(m).wait_send()
+            loop(1, n_tp, lambda k: t2_copy(m, k).wait_send())
+        t3_copy(m).wait_send()
     loop(0, n_z, lambda kz: o_copy(kz).wait_send())
     for m in order[:-1]:
         z_copy(m).wait_send()
@@ -352,7 +376,7 @@
                 dma((2,)), dma((2, slots)), dma((n_chunks,)), dma((2, n_chunks)), dma((n_chunks,)),
             ] + [dma(shape) for shape in pairs for _ in range(2)],
             compiler_params=pltpu.CompilerParams(collective_id=0, has_side_effects=True),
-        )(tokens, experts, routing, lines, gate_master, linear_master, down_weight)
+        )(tokens, experts.T, routing.T, lines, gate_master, linear_master, down_weight)
 
     placed = (
         P("fs", None),

time: 147 us -> 136 us (0.925)
  Pallas kernels: 138 us -> 130 us
  local copies, waits for them, and re-layouts: 8.01 us -> 5.18 us
    pallas_call x1, Pallas kernels: 138 us -> 130 us  [on_device(): pl.pallas_call(functools.partial(kernel, n_fs, n_tp, n_chunks), out_shape...]
    unnamed x9 -> x7, local copies, waits for them, and re-layouts: 8.01 us -> 5.18 us
where the time goes in v4:
time: 136 us; the launch traced here: 135 us
  Pallas kernels  130 us (96%)
  local copies, waits for them, and re-layouts  5.18 us (4%)
    pallas_call x1, Pallas kernels, on_device(): pl.pallas_call(functools.partial(kernel, n_fs, n_tp, n_chunks), out_shape...  130 us
    unnamed x7, local copies, waits for them, and re-layouts  5.18 us

profile of v4, /device:TPU:0, one launch (start us, length us, event | category | flops | bytes accessed | tf_op | source)
XLA Modules:
  0.0 135.5 jit_solution(4779044812029893417)
XLA Ops:
  0.6 129.7 %shard_map.94 = (bf16[1,2048,512]{2,1,0:T(8,128)(2,1)}, bf16[1,2048,512]{2,1,0:T(8,128)(2,1)}, bf16[128,512]{1,0:T(8,128)(2,1)}) custom-call(bf16[128,2048]{1,0:T(8,128)(2,1)} %tokens_ref.1, s32[4,128]{1,0:T(4,128)} %bitcast.4, f32[4,128]{1,0:T(4,128)} %bitcast.5, f32[16,128]{1,0:T(8,128)} %bitcast.3, f32[8,256,512]{2,1,0:T(8,128)} %gate_ref.1, ...), custom_call_target="tpu_custom_call" | custom-call | tf_op jit(solution)/shard_map/pallas_call | solution.py:356
  130.3 0.0 copy-start
  130.3 3.2 %copy.13 = bf16[1,2048,512]{2,1,0:T(8,128)(2,1)} copy(bf16[1,2048,512]{2,1,0:T(8,128)(2,1)} %get-tuple-element.6) | data formatting | bytes 4194304
  133.5 0.0 copy-done
  133.5 0.0 copy-start.1
  133.5 1.3 copy.14
  134.8 0.0 copy-done.1
  134.8 0.7 copy.15
Async XLA Ops:
  130.3 3.2 %copy-start = (bf16[1,2048,512]{2,1,0:T(8,128)(2,1)S(1)}, bf16[1,2048,512]{2,1,0:T(8,128)(2,1)}, u32[]{:S(2)}) copy-start(bf16[1,2048,512]{2,1,0:T(8,128)(2,1)} %get-tuple-element.7) | copy-start | bytes 6291460
  133.5 1.3 copy-start.1

commit v5 on v4

--- a/solution.py
+++ b/solution.py
@@ -31,7 +31,7 @@
     osend, orecv, zsend, zrecv,
     local_sem, stage_sem, own_sem, out_sem, dl_sem,
     w_s, w_r, s_s, s_r, t1_s, t1_r, t2_s, t2_r, t3_s, t3_r,
-    d_s, d_r, a_s, a_r, l_s, l_r, o_s, o_r, z_s, z_r,
+    d_s, d_r, a_s, a_r, o_s, o_r, z_s, z_r,
 ):
     fs, tp = lax.axis_index("fs"), lax.axis_index("tp")
     n_z = n_fs // CORES
@@ -120,10 +120,6 @@
             down_ref.at[0, ds(tp, dcols), pl.ds(j * ch, ch)], dts.at[j, :, ds(tp, ch)], dl_sem.at[j]
         )
 
-    def a_copy(j, k):
-        block = acts.at[j, :, ds(tp, ch)]
-        return remote(block, block, a_s.at[j, k], a_r.at[j, k], peer_tp(k))
-
     def outs(j):
         c = pl.ds(j * ch, ch)
         return (
@@ -134,9 +130,9 @@
     def o_copy(kz):
         return remote(osend.at[kz], orecv.at[kz], o_s.at[kz], o_r.at[kz], over)
 
-    def l_copy(m, k):
-        block = acts.at[n_chunks - 1, ds(zx(m), CORES * tok), ds(tp, ch)]
-        return remote(block, block, l_s.at[m, k], l_r.at[m, k], peer_tp(k))
+    def a_copy(j, m, k):
+        block = acts.at[j, ds(zx(m), CORES * tok), ds(tp, ch)]
+        return remote(block, block, a_s.at[j, m, k], a_r.at[j, m, k], peer_tp(k))
 
     def z_copy(m):
         where = {"fs": zx(m) * CORES + core, "tp": tp}
@@ -205,11 +201,14 @@
     t3_copy(0).start()
     for m in range(1, across):
         spread(m)
-    for j in range(1, n_chunks):
-        prepare(j)
-    for j in range(1, n_chunks):
-        for k in crossing:
-            w_copy(j, k).start()
+    for js in ([1], list(range(2, n_chunks))):
+        for j in js:
+            if j < n_chunks:
+                prepare(j)
+        for j in js:
+            for k in crossing:
+                if j < n_chunks:
+                    w_copy(j, k).start()
     for m in range(across + 1, n_z):
         spread(m)
     for j in range(early, n_chunks):
@@ -227,16 +226,19 @@
     def down(j):
         d_own(j).wait()
         loop(1, n_tp, lambda k: d_copy(j, k).wait_recv())
-        if j < n_chunks - 1:
-            loop(1, n_tp, lambda k: a_copy(j, k).wait_recv())
 
     def product(j, r):
         return lax.dot_general(
             acts[j, r, :], dts[j], (((1,), (1,)), ((), ())), preferred_element_type=F32
         )
 
+    def gathered(j, m):
+        loop(1, n_tp, lambda k: a_copy(j, m, k).wait_recv())
+
     def accumulate(j):
         down(j)
+        for m in range(n_z):
+            gathered(j, m)
 
         def step(i, carry):
             r = ds(i, rows)
@@ -262,14 +264,14 @@
         acts[j, r, ds(tp, ch)] = (c * jax.nn.sigmoid(gate_slope * c) * lin).astype(BF16)
 
     last = n_chunks - 1
-    for j in range(last):
+    order = list(range(n_z - 1, -1, -1))
+    for j in range(n_chunks):
         arrive(j)
-        lax.fori_loop(0, total // rows, lambda i, c: (up(j, ds(i, rows)), c)[1], 0)
-        loop(1, n_tp, lambda k: a_copy(j, k).start())
+        for m in order:
+            up(j, ds(zx(m), CORES * tok))
+            loop(1, n_tp, lambda k: a_copy(j, m, k).start())
         if j > 0:
             accumulate(j - 1)
-    if last > 0:
-        accumulate(last - 1)
 
     loop(1, n_fs, lambda k: s_copy(k).wait_recv())
     down(last)
@@ -292,13 +294,8 @@
             zsend[m] = (acc[r, :] + orecv[m].astype(F32)).astype(BF16)
             z_copy(m).start()
 
-    order = list(range(n_z - 1, -1, -1))
-    arrive(last)
     for m in order:
-        up(last, ds(zx(m), CORES * tok))
-        loop(1, n_tp, lambda k: l_copy(m, k).start())
-    for m in order:
-        loop(1, n_tp, lambda k: l_copy(m, k).wait_recv())
+        gathered(last, m)
         osend[m] = weighted(zx(m) * CORES + (1 - core)).astype(BF16)
         o_copy(m).start()
         kept = zx(m) * CORES + core
@@ -318,10 +315,8 @@
         for k in range(1, n_fs):
             w_copy(j, k).wait_send()
         loop(1, n_tp, lambda k: d_copy(j, k).wait_send())
-        if j < last:
-            loop(1, n_tp, lambda k: a_copy(j, k).wait_send())
-    for m in order:
-        loop(1, n_tp, lambda k: l_copy(m, k).wait_send())
+        for m in order:
+            loop(1, n_tp, lambda k: a_copy(j, m, k).wait_send())
     loop(1, n_fs, lambda k: s_copy(k).wait_send())
     for m in range(n_z):
         if m > 0:
@@ -351,7 +346,7 @@
         out_shape = jax.ShapeDtypeStruct((1, width, cols), BF16)
         pairs = [
             (n_chunks, n_fs), (n_fs,), (n_z,), (n_z, n_tp), (n_z,),
-            (n_chunks, n_tp), (n_chunks, n_tp), (n_z, n_tp), (n_z,), (n_z,),
+            (n_chunks, n_tp), (n_chunks, n_z, n_tp), (n_z,), (n_z,),
         ]
         return pl.pallas_call(
             functools.partial(kernel, n_fs, n_tp, n_chunks),

time: 136 us -> 132 us (0.971)
  Pallas kernels: 130 us -> 126 us
    pallas_call x1, Pallas kernels: 130 us -> 126 us  [on_device(): pl.pallas_call(functools.partial(kernel, n_fs, n_tp, n_chunks), out_shape...]
where the time goes in v5:
time: 132 us
  Pallas kernels  126 us (95%)
  local copies, waits for them, and re-layouts  5.18 us (4%)
    pallas_call x1, Pallas kernels, on_device(): pl.pallas_call(functools.partial(kernel, n_fs, n_tp, n_chunks), out_shape...  126 us
    unnamed x7, local copies, waits for them, and re-layouts  5.18 us

profile of v5, /device:TPU:0, one launch (start us, length us, event | category | flops | bytes accessed | tf_op | source)
XLA Modules:
  0.0 131.6 jit_solution(8450463254447337117)
XLA Ops:
  0.6 125.7 %shard_map.94 = (bf16[1,2048,512]{2,1,0:T(8,128)(2,1)}, bf16[1,2048,512]{2,1,0:T(8,128)(2,1)}, bf16[128,512]{1,0:T(8,128)(2,1)}) custom-call(bf16[128,2048]{1,0:T(8,128)(2,1)} %tokens_ref.1, s32[4,128]{1,0:T(4,128)} %bitcast.4, f32[4,128]{1,0:T(4,128)} %bitcast.5, f32[16,128]{1,0:T(8,128)} %bitcast.3, f32[8,256,512]{2,1,0:T(8,128)} %gate_ref.1, ...), custom_call_target="tpu_custom_call" | custom-call | tf_op jit(solution)/shard_map/pallas_call | solution.py:351
  126.4 0.0 copy-start
  126.4 3.2 %copy.13 = bf16[1,2048,512]{2,1,0:T(8,128)(2,1)} copy(bf16[1,2048,512]{2,1,0:T(8,128)(2,1)} %get-tuple-element.6) | data formatting | bytes 4194304
  129.6 0.0 copy-done
  129.6 0.0 copy-start.1
  129.6 1.3 %copy.14 = bf16[1,2048,512]{2,1,0:T(8,128)(2,1)} copy(bf16[1,2048,512]{2,1,0:T(8,128)(2,1)S(1)} %copy-done) | data formatting | bytes 4194304
  130.9 0.0 copy-done.1
  130.9 0.7 copy.15
Async XLA Ops:
  126.4 3.2 %copy-start = (bf16[1,2048,512]{2,1,0:T(8,128)(2,1)S(1)}, bf16[1,2048,512]{2,1,0:T(8,128)(2,1)}, u32[]{:S(2)}) copy-start(bf16[1,2048,512]{2,1,0:T(8,128)(2,1)} %get-tuple-element.7) | copy-start | bytes 6291460
  129.6 1.3 %copy-start.1 = (bf16[128,512]{1,0:T(8,128)(2,1)S(1)}, bf16[128,512]{1,0:T(8,128)(2,1)}, u32[]{:S(2)}) copy-start(bf16[128,512]{1,0:T(8,128)(2,1)} %get-tuple-element.8) | copy-start | bytes 393220
